TPU v7x, 128 devices: a whole 4x4x4 slice. The times are simulated.
128 devices in a mesh: sp: 64 (over z, y, x), tp: 2 (over core).
Axes of the slice: x: 4, y: 4, z: 4, core: 2. Of those that a mesh axis runs over, the one named last changes fastest.
Arguments:
- gate_pre: bfloat16 [16384, 2048], P('sp', 'tp'), may hold values from -6 to 6
- conv_in: bfloat16 [16384, 2048], P('sp', 'tp'), may hold values from -6 to 6
- conv_taps: bfloat16 [4, 2048], P(None, 'tp'), may hold values from -3 to 3
- recur_map: bfloat16 [8, 256, 256], P('tp'), may hold values from -0.375 to 0.375
- input_map: bfloat16 [8, 256, 256], P('tp'), may hold values from -0.375 to 0.375
- rate_logit: float32 [2048], P('tp'), may hold values from 4.5 to 15
- decay_shift: float32 [16384, 8], P('sp', 'tp'), may hold values from -1.5 to 0
- out_weight: bfloat16 [2048, 2048], replicated, may hold values from -0.25 to 0.25
- residual: bfloat16 [16384, 2048], P(('sp', 'tp')), may hold values from -6 to 6
- gain_mix: float32 [2048], replicated, may hold values from 0.1 to 1.9
- routes: int32 [16384, 4], P(('sp', 'tp')), may hold values from 0 to 127, all different within a row; in each aligned block of 128 rows (0 to 127, 128 to 255, ...) at most 8 rows name the same one
- route_weight: float32 [16384, 4], P(('sp', 'tp')), may hold values from 0.2 to 1
- shared_gate: bfloat16 [2048, 512], replicated, may hold values from -0.125 to 0.125
- shared_up: bfloat16 [2048, 512], replicated, may hold values from -0.125 to 0.125
- shared_down: bfloat16 [512, 2048], replicated, may hold values from -0.375 to 0.375
- expert_gate: bfloat16 [128, 2048, 512], P(('sp', 'tp')), may hold values from -0.125 to 0.125
- expert_up: bfloat16 [128, 2048, 512], P(('sp', 'tp')), may hold values from -0.125 to 0.125
- expert_down: bfloat16 [128, 512, 2048], P(('sp', 'tp')), may hold values from -0.375 to 0.375
- gain_out: float32 [2048], replicated, may hold values from 0.1 to 1.9
Outputs:
- layer_out: bfloat16 [16384, 2048], P(('sp', 'tp'))
Inputs may be any that keep to these rules, and one draw needn't show every extreme that they name: `routes`: each row names 4 different experts. In the rows of one device (aligned blocks of 128 rows) no expert is named more than 8 times, and in some blocks one expert is named exactly 8 times.
All inputs are finite; a program needn't handle non-finite values.
Results may differ from a plain program's by a relative error of at most 0.014.
Values may be sent and summed in bfloat16 or wider, within the bound.
A program may use at most 128 MiB of HBM per device.

v0:
```python
import jax
import jax.numpy as jnp
from jax import lax
from jax.sharding import PartitionSpec as P

ALPHA = 8.0**0.25
RATE_C = 8.0
NORM_EPS = 1e-05


def from_behind(block, axis, distance):
    devices = range(lax.axis_size(axis))
    route = [(i - distance, i) for i in devices if i - distance in devices]
    return lax.ppermute(block, axis, route)


def sent_to_all(x, axis):
    count = lax.axis_size(axis)
    return lax.all_to_all(jnp.broadcast_to(x[None], (count, *x.shape)), axis, 0, 0, tiled=True)


def gathered_once(x, axis):
    leaves = jax.tree.leaves(x)
    order = sorted(range(len(leaves)), key=lambda k: -leaves[k].size)
    width = (1, *leaves[order[0]].shape)[-1]
    lines = [
        jnp.pad(leaves[k].reshape(-1), (0, -leaves[k].size % width)).reshape(-1, width)
        for k in order
    ]
    both, at, found = (sent_to_all(jnp.concatenate(lines), axis), 0, {})
    for k, line in zip(order, lines):
        slab = both[:, at : at + len(line)].reshape(len(both), -1)
        found[k] = slab[:, : leaves[k].size].reshape(-1, *leaves[k].shape)
        at += len(line)
    numbers = iter(range(len(leaves)))
    return jax.tree.map(lambda _: found[next(numbers)], x)


def folded_in_pairs(pieces, combine):
    while len(jax.tree.leaves(pieces)[0]) > 1:
        pieces = jax.vmap(combine)(
            *(jax.tree.map(lambda part: part[side::2], pieces) for side in (0, 1))
        )
    return jax.tree.map(lambda part: part[0], pieces)


def entering(x, axis, combine, identity):
    count, here = (lax.axis_size(axis), lax.axis_index(axis))
    passed = jnp.arange(count) < here

    def kept(part, zero, own):
        part = jnp.where(
            passed.reshape(-1, *(1 for _ in own.shape)), part, jnp.asarray(zero, own.dtype)
        )
        return part

    pieces = gathered_once(x, axis)
    return folded_in_pairs(jax.tree.map(kept, pieces, identity, x), combine)


def layer_norm(values, gains):
    center = values - jnp.mean(values, axis=-1, keepdims=True)
    spread = jnp.mean(center * center, axis=-1, keepdims=True)
    return center * lax.rsqrt(spread + NORM_EPS) * gains


def combine(former, latter):
    return (former[0] * latter[0], latter[0] * former[1] + latter[1])


def on_device(
    gate_pre,
    conv_in,
    conv_taps,
    recur_map,
    input_map,
    rate_logit,
    decay_shift,
    out_weight,
    residual,
    gain_mix,
    routes,
    route_weight,
    shared_gate,
    shared_up,
    shared_down,
    expert_gate,
    expert_up,
    expert_down,
    gain_out,
):
    tokens, channels = conv_in.shape
    reach = conv_taps.shape[0] - 1
    head_count, head_width = (recur_map.shape[0], recur_map.shape[1])
    before = from_behind(conv_in[tokens - reach :], "sp", 1)
    extended = jnp.concatenate([before, conv_in], axis=0).astype(jnp.float32)
    filter_tap_weight = conv_taps.astype(jnp.float32)
    summed = jnp.zeros((tokens, channels), jnp.float32)
    for offset in range(reach + 1):
        summed = summed + filter_tap_weight[offset] * extended[offset : offset + tokens]
    conv_out = summed.astype(jnp.bfloat16).reshape(tokens, head_count, head_width)
    recur_gate = jax.nn.sigmoid(
        jnp.einsum("thc,hcd->thd", conv_out, recur_map, preferred_element_type=jnp.float32)
    )
    input_gate = jax.nn.sigmoid(
        jnp.einsum("thc,hcd->thd", conv_out, input_map, preferred_element_type=jnp.float32)
    )
    log_decay = (
        -RATE_C * jax.nn.softplus(-rate_logit).reshape(head_count, head_width) * recur_gate
        + decay_shift[:, :, None]
    )
    update = jnp.sqrt(-jnp.expm1(2.0 * log_decay)) * input_gate * conv_out.astype(jnp.float32)
    running, local_state = lax.associative_scan(combine, (jnp.exp(log_decay), update), axis=0)
    carried = entering(
        (running[-1], local_state[-1]),
        "sp",
        combine,
        (jnp.ones_like(running[-1]), jnp.zeros_like(local_state[-1])),
    )
    states = local_state + running * carried[1][None]
    mixed_rows = (
        states.reshape(tokens, channels)
        * jax.nn.gelu(gate_pre.astype(jnp.float32), approximate=True)
    ).astype(jnp.bfloat16)
    row_count = tokens // lax.axis_size("tp")
    regrouped = lax.all_to_all(mixed_rows, "tp", split_axis=0, concat_axis=1, tiled=True)
    projected = jnp.dot(regrouped, out_weight, preferred_element_type=jnp.float32)
    normed = layer_norm(ALPHA * residual.astype(jnp.float32) + projected, gain_mix).astype(
        jnp.bfloat16
    )
    model_width = normed.shape[1]
    fanout = routes.shape[1]
    sp_count, tp_count = (lax.axis_size("sp"), lax.axis_size("tp"))
    experts = sp_count * tp_count
    capacity = max(2, 2 * row_count * fanout // experts)
    entries = row_count * fanout
    flat_ids = routes.reshape(entries)
    onehot = (flat_ids[:, None] == lax.iota(jnp.int32, experts)[None, :]).astype(jnp.bfloat16)
    before_mask = (
        lax.iota(jnp.int32, entries)[:, None] > lax.iota(jnp.int32, entries)[None, :]
    ).astype(jnp.bfloat16)
    earlier = jnp.dot(before_mask, onehot, preferred_element_type=jnp.float32)
    slot_rank = jnp.sum(earlier * onehot.astype(jnp.float32), axis=1).astype(jnp.int32)
    slot_index = flat_ids * capacity + slot_rank
    source_row = (
        jnp.full((experts * capacity,), row_count, jnp.int32)
        .at[slot_index]
        .set(lax.iota(jnp.int32, entries) // fanout)
    )
    padded_rows = jnp.concatenate([normed, jnp.zeros((1, model_width), jnp.bfloat16)], axis=0)
    outgoing = padded_rows[source_row].reshape(experts, capacity, model_width)
    shared_hidden = (
        jax.nn.silu(jnp.dot(normed, shared_gate, preferred_element_type=jnp.float32))
        * jnp.dot(normed, shared_up, preferred_element_type=jnp.float32)
    ).astype(jnp.bfloat16)
    shared_out = jnp.dot(shared_hidden, shared_down, preferred_element_type=jnp.float32)
    received = lax.all_to_all(outgoing, ("sp", "tp"), split_axis=0, concat_axis=0, tiled=True)
    senders = received.shape[0]
    slot_count = received.shape[1]
    chosen = received.reshape(senders * slot_count, model_width)
    hidden = (
        jax.nn.silu(jnp.dot(chosen, expert_gate[0], preferred_element_type=jnp.float32))
        * jnp.dot(chosen, expert_up[0], preferred_element_type=jnp.float32)
    ).astype(jnp.bfloat16)
    handed_result = lax.all_to_all(
        jnp.dot(hidden, expert_down[0], preferred_element_type=jnp.float32)
        .astype(jnp.bfloat16)
        .reshape(senders, slot_count, model_width),
        ("sp", "tp"),
        split_axis=0,
        concat_axis=0,
        tiled=True,
    )
    gathered = handed_result.reshape(experts * capacity, model_width)[slot_index].reshape(
        row_count, fanout, model_width
    )
    moe_sum = shared_out + jnp.sum(route_weight[:, :, None] * gathered.astype(jnp.float32), axis=1)
    return layer_norm(ALPHA * normed.astype(jnp.float32) + moe_sum, gain_out).astype(jnp.bfloat16)


def solution(mesh):
    return jax.shard_map(
        on_device,
        mesh=mesh,
        in_specs=(
            P("sp", "tp"),
            P("sp", "tp"),
            P(None, "tp"),
            P("tp", None, None),
            P("tp", None, None),
            P("tp"),
            P("sp", "tp"),
            P(),
            P(("sp", "tp"), None),
            P(),
            P(("sp", "tp"), None),
            P(("sp", "tp"), None),
            P(),
            P(),
            P(),
            P(("sp", "tp"), None, None),
            P(("sp", "tp"), None, None),
            P(("sp", "tp"), None, None),
            P(),
        ),
        out_specs=P(("sp", "tp"), None),
        check_vma=False,
    )
```

profile of v0, /device:TPU:3, one launch (start us, length us, event | category | flops | bytes accessed | tf_op | source)
XLA Modules:
  0.0 345.6 jit_solution(3061634568221742398)
XLA Ops:
  1.8 3.1 collective-permute-start
  20.3 3.3 slice.353
  23.6 3.3 slice.354
  90.8 3.3 slice.408
  94.1 3.3 slice.351
  108.7 4.3 %pad.130 = f32[256,4,256]{2,0,1:T(8,128)} pad(f32[128,4,256]{2,0,1:T(8,128)} %add.316, f32[]{:T(128)} %constant.23.clone.1), padding=1_0_1x0_0_0x0_0_0 | pad | bytes 1572868 | tf_op jit(solution)/shard_map/pad | solution.py:113
  114.6 3.9 %pad.111 = f32[128,4,256]{2,0,1:T(8,128)} pad(f32[64,4,256]{2,0,1:T(8,128)} %pad_maximum_fusion.2, f32[]{:T(128)} %constant.23.clone.1), padding=0_1_1x0_0_0x0_0_0 | pad | bytes 786436 | tf_op jit(solution)/shard_map/pad | solution.py:113
  126.1 4.3 %pad.129 = f32[256,4,256]{2,0,1:T(8,128)} pad(f32[128,4,256]{2,0,1:T(8,128)} %pad_maximum_fusion.1, f32[]{:T(128)} %constant.23.clone.1), padding=0_1_1x0_0_0x0_0_0 | pad | bytes 1572868 | tf_op jit(solution)/shard_map/pad | solution.py:113
  131.2 4.3 %pad.114 = f32[256,4,256]{2,0,1:T(8,128)} pad(f32[128,4,256]{2,0,1:T(8,128)} %add.307, f32[]{:T(128)} %constant.23.clone.1), padding=1_0_1x0_0_0x0_0_0 | pad | bytes 1572868 | tf_op jit(solution)/shard_map/pad | solution.py:113
  137.3 4.3 %pad.113 = f32[256,4,256]{2,0,1:T(8,128)} pad(f32[128,4,256]{2,0,1:T(8,128)} %pad_maximum_fusion, f32[]{:T(128)} %constant.23.clone.1), padding=0_1_1x0_0_0x0_0_0 | pad | bytes 1572868 | tf_op jit(solution)/shard_map/pad | solution.py:113
  143.3 10.8 %all-to-all-start = ((f32[64,8,256]{2,1,0:T(8,128)}), f32[64,8,256]{2,1,0:T(8,128)}, u32[]{:S(2)}, u32[]{:S(2)}) async-start(f32[64,8,256]{2,1,0:T(8,128)} %broadcast_in_dim.25), calls=%async_computation | async-start | bytes 1048576 | tf_op jit(solution)/shard_map/all_to_all | solution.py:19
  157.0 8.2 %all-to-all-done = f32[64,8,256]{2,1,0:T(8,128)} async-done(((f32[64,8,256]{2,1,0:T(8,128)}), f32[64,8,256]{2,1,0:T(8,128)}, u32[]{:S(2)}, u32[]{:S(2)}) %all-to-all-start) | async-done | bytes 524320 | tf_op jit(solution)/shard_map/all_to_all | solution.py:19
  172.7 6.3 %all_to_all.34 = bf16[2,128,1024]{1,2,0:T(8,128)(2,1)S(1)} all-to-all(bf16[2,128,1024]{1,2,0:T(8,128)(2,1)S(1)} %copy_bitcast_fusion), channel_id=1, replica_groups=mesh['sp'=64,'tp'=2] {'tp'}, dimensions={0} | all-to-all | bytes 1048576 | tf_op jit(solution)/shard_map/all_to_all | solution.py:126
  179.0 4.8 %fusion.75 = (f32[128]{0:T(128)S(1)}, f32[128,2048]{1,0:T(8,128)S(1)}) fusion(bf16[128,2048]{0,1:T(8,128)(2,1)S(1)} %bitcast.85, bf16[2048,2048]{1,0:T(8,128)(2,1)} %param.26, bf16[128,2048]{1,0:T(8,128)(2,1)S(1)} %copy-done.9), kind=kOutput, calls=%fused_computation.171 | convolution fusion | flops 1074790272 | bytes 10486272 | tf_op jit(solution)/shard_map/dot_general | solution.py:127
  184.3 6.0 %gather_fusion = bf16[1024,2048]{1,0:T(8,128)(2,1)} fusion(bf16[129,2048]{1,0:T(8,128)(2,1)S(1)} %concatenate.67, s32[1024]{0:T(1024)S(1)} %fusion.61), kind=kCustom, calls=%fused_computation | custom fusion | bytes 8392704 | tf_op jit(solution)/shard_map/gather | solution.py:151
  190.4 57.0 %all_to_all.35 = bf16[128,8,2048]{2,1,0:T(8,128)(2,1)S(1)} all-to-all(bf16[128,8,2048]{2,1,0:T(8,128)(2,1)} %bitcast.84), channel_id=1, replica_groups=mesh['sp'=64,'tp'=2] {'sp','tp'}, dimensions={0} | all-to-all | bytes 8388608 | tf_op jit(solution)/shard_map/all_to_all | solution.py:157
  249.4 3.6 %fusion.2 = f32[1024,512]{1,0:T(8,128)} fusion(bf16[128,8,2048]{2,1,0:T(8,128)(2,1)S(1)} %all_to_all.35, bf16[1,2048,512]{2,1,0:T(8,128)(2,1)S(1)} %copy-done.39), kind=kOutput, calls=%fused_computation.5 | convolution fusion | flops 2147483648 | bytes 8388608 | tf_op jit(solution)/shard_map/dot_general | solution.py:162
  253.0 10.0 %convert_bitcast_fusion = bf16[128,8,2048]{2,1,0:T(8,128)(2,1)} fusion(bf16[1,512,2048]{2,1,0:T(8,128)(2,1)S(1)} %copy-done, f32[1024,512]{1,0:T(8,128)} %fusion.2, bf16[1,2048,512]{2,1,0:T(8,128)(2,1)} %param.35, bf16[128,8,2048]{2,1,0:T(8,128)(2,1)} %copy-done.5), kind=kOutput, calls=%fused_computation.8 | convolution fusion | flops 4300210176 | bytes 14680064 | tf_op jit(solution)/shard_map/dot_general | solution.py:166
  263.0 7.0 %all-to-all-start.3 = ((bf16[128,8,2048]{2,1,0:T(8,128)(2,1)}), bf16[128,8,2048]{2,1,0:T(8,128)(2,1)}, u32[]{:S(2)}, u32[]{:S(2)}) async-start(bf16[128,8,2048]{2,1,0:T(8,128)(2,1)} %convert_bitcast_fusion), calls=%async_computation.3 | async-start | bytes 8388608 | tf_op jit(solution)/shard_map/all_to_all | solution.py:165
  272.3 49.2 %all-to-all-done.3 = bf16[128,8,2048]{2,1,0:T(8,128)(2,1)} async-done(((bf16[128,8,2048]{2,1,0:T(8,128)(2,1)}), bf16[128,8,2048]{2,1,0:T(8,128)(2,1)}, u32[]{:S(2)}, u32[]{:S(2)}) %all-to-all-start.3) | async-done | bytes 4194336 | tf_op jit(solution)/shard_map/all_to_all | solution.py:165
  321.4 7.9 %gather_fusion.1 = bf16[512,2048]{1,0:T(8,128)(2,1)} fusion(bf16[1024,2048]{1,0:T(8,128)(2,1)} %bitcast.20, s32[1024]{0:T(1024)S(1)} %pad_clamp_fusion), kind=kCustom, calls=%fused_computation.1 | custom fusion | bytes 4196352 | tf_op jit(solution)/shard_map/gather | solution.py:174
  329.4 4.7 %reshape.117 = f32[128,4,2048]{2,1,0:T(4,128)} reshape(bf16[512,2048]{1,0:T(8,128)(2,1)} %gather_fusion.1) | data formatting | bytes 6291456 | tf_op jit(solution)/shard_map/convert_element_type | solution.py:177
  334.1 6.3 %multiply_reduce_fusion = f32[128,2048]{1,0:T(8,128)} fusion(f32[128,4,2048]{2,1,0:T(4,128)} %reshape.117, f32[128,4]{1,0:T(8,128)S(1)} %copy.31), kind=kLoop, calls=%fused_computation.7 | loop fusion | flops 1835008 | bytes 5244928 | tf_op jit(solution)/shard_map/reduce_sum | solution.py:177
  340.5 3.8 %fusion.76 = (f32[128]{0:T(128)S(1)}, f32[128,2048]{1,0:T(8,128)S(1)}) fusion(f32[128,2048]{1,0:T(8,128)} %multiply_reduce_fusion, bf16[512,2048]{1,0:T(8,128)(2,1)} %param.33, bf16[128,2048]{1,0:T(8,128)(2,1)} %copy-done.1, bf16[2048,512]{1,0:T(8,128)(2,1)} %param.32, f32[128,512]{1,0:T(8,128)S(1)} %fusion.77), kind=kOutput, calls=%fused_computation.172 | convolution fusion | flops 538574720 | bytes 7078400 | tf_op jit(solution)/shard_map/dot_general | solution.py:156
  (250 shorter events, 121.7 us)
Async XLA Ops:
  0.0 253.0 %copy-start = (bf16[1,512,2048]{2,1,0:T(8,128)(2,1)S(1)}, bf16[1,512,2048]{2,1,0:T(8,128)(2,1)}, u32[]{:S(2)}) copy-start(bf16[1,512,2048]{2,1,0:T(8,128)(2,1)} %param.36) | copy-start | bytes 6291460
  0.0 10.2 %copy-start.10 = (bf16[256,1024]{1,0:T(8,128)(2,1)S(1)}, bf16[256,1024]{1,0:T(8,128)(2,1)}, u32[]{:S(2)}) copy-start(bf16[256,1024]{1,0:T(8,128)(2,1)} %param.19) | copy-start | bytes 1572868
  1.8 10.8 %collective-permute-start = (bf16[3,1024]{0,1:T(8,128)(2,1)}, bf16[3,1024]{0,1:T(8,128)(2,1)S(1)}, u32[]{:S(2)}, u32[]{:S(2)}) collective-permute-start(bf16[3,1024]{0,1:T(8,128)(2,1)} %copy.22), channel_id=1, source_target_pairs={{0,2},{2,4},{4,6},{6,8},{8,10},{10,12},{12,14},{14,16},{16,18},{18... | collective-permute-start | bytes 18440 | tf_op jit(solution)/shard_map/ppermute | solution.py:14
  87.9 12.1 %copy-start.19 = (f32[2,4,256]{2,0,1:T(2,128)S(1)}, f32[2,4,256]{2,0,1:T(2,128)}, u32[]{:S(2)}) copy-start(f32[2,4,256]{2,0,1:T(2,128)} %get-tuple-element.63) | copy-start | bytes 24580
  87.9 12.2 %copy-start.18 = (f32[2,4,256]{2,0,1:T(2,128)S(1)}, f32[2,4,256]{2,0,1:T(2,128)}, u32[]{:S(2)}) copy-start(f32[2,4,256]{2,0,1:T(2,128)} %get-tuple-element.62) | copy-start | bytes 24580
  87.9 12.2 %copy-start.30 = (f32[1,4,256]{2,0,1:T(1,128)S(1)}, f32[1,4,256]{2,0,1:T(1,128)}, u32[]{:S(2)}) copy-start(f32[1,4,256]{2,0,1:T(1,128)} %get-tuple-element.40) | copy-start | bytes 12292
  87.9 12.2 %copy-start.31 = (f32[1,4,256]{2,0,1:T(1,128)S(1)}, f32[1,4,256]{2,0,1:T(1,128)}, u32[]{:S(2)}) copy-start(f32[1,4,256]{2,0,1:T(1,128)} %get-tuple-element.41) | copy-start | bytes 12292
  87.9 12.2 %copy-start.32 = (f32[1,4,256]{2,0,1:T(1,128)S(1)}, f32[1,4,256]{2,0,1:T(1,128)}, u32[]{:S(2)}) copy-start(f32[1,4,256]{2,0,1:T(1,128)} %get-tuple-element.42) | copy-start | bytes 12292
  88.0 12.2 %copy-start.33 = (f32[1,4,256]{2,0,1:T(1,128)S(1)}, f32[1,4,256]{2,0,1:T(1,128)}, u32[]{:S(2)}) copy-start(f32[1,4,256]{2,0,1:T(1,128)} %get-tuple-element.43) | copy-start | bytes 12292
  88.0 12.7 %copy-start.15 = (f32[7,4,256]{2,0,1:T(8,128)S(1)}, f32[7,4,256]{2,0,1:T(8,128)}, u32[]{:S(2)}) copy-start(f32[7,4,256]{2,0,1:T(8,128)} %slice.375) | copy-start | bytes 86020
  88.0 12.7 %copy-start.16 = (f32[7,4,256]{2,0,1:T(8,128)S(1)}, f32[7,4,256]{2,0,1:T(8,128)}, u32[]{:S(2)}) copy-start(f32[7,4,256]{2,0,1:T(8,128)} %slice.400) | copy-start | bytes 86020
  89.6 12.8 %copy-start.13 = (f32[15,4,256]{2,0,1:T(8,128)S(1)}, f32[15,4,256]{2,0,1:T(8,128)}, u32[]{:S(2)}) copy-start(f32[15,4,256]{2,0,1:T(8,128)} %slice.369) | copy-start | bytes 184324
  89.6 12.8 %copy-start.14 = (f32[15,4,256]{2,0,1:T(8,128)S(1)}, f32[15,4,256]{2,0,1:T(8,128)}, u32[]{:S(2)}) copy-start(f32[15,4,256]{2,0,1:T(8,128)} %slice.402) | copy-start | bytes 184324
  90.2 10.2 %copy-start.17 = (f32[3,4,256]{2,0,1:T(4,128)S(1)}, f32[3,4,256]{2,0,1:T(4,128)}, u32[]{:S(2)}) copy-start(f32[3,4,256]{2,0,1:T(4,128)} %slice.398) | copy-start | bytes 36868
  90.2 10.3 %copy-start.29 = (f32[1,4,256]{2,0,1:T(1,128)S(1)}, f32[1,4,256]{2,0,1:T(1,128)}, u32[]{:S(2)}) copy-start(f32[1,4,256]{2,0,1:T(1,128)} %slice.494) | copy-start | bytes 12292
  90.2 10.4 %copy-start.28 = (f32[1,4,256]{2,0,1:T(1,128)S(1)}, f32[1,4,256]{2,0,1:T(1,128)}, u32[]{:S(2)}) copy-start(f32[1,4,256]{2,0,1:T(1,128)} %slice.468) | copy-start | bytes 12292
  90.8 11.6 %copy-start.27 = (f32[1,4,256]{2,0,1:T(1,128)S(1)}, f32[1,4,256]{2,0,1:T(1,128)}, u32[]{:S(2)}) copy-start(f32[1,4,256]{2,0,1:T(1,128)} %slice.492) | copy-start | bytes 12292
  125.3 10.2 %copy-start.20 = (f32[1,4,256]{2,0,1:T(1,128)S(1)}, f32[1,4,256]{2,0,1:T(1,128)}, u32[]{:S(2)}) copy-start(f32[1,4,256]{2,0,1:T(1,128)} %slice.463) | copy-start | bytes 12292
  135.4 18.7 %copy-start.36 = (s32[512,1]{0,1:T(1,128)S(1)}, s32[512,1]{0,1:T(1,128)}, u32[]{:S(2)}) copy-start(s32[512,1]{0,1:T(1,128)} %mul.400) | copy-start | bytes 6148
  135.4 18.7 %copy-start.37 = (s32[512]{0:T(512)S(1)}, s32[512]{0:T(512)}, u32[]{:S(2)}) copy-start(s32[512]{0:T(512)} %convert_element_type.77) | copy-start | bytes 6148
  143.3 21.9 %all-to-all-start = ((f32[64,8,256]{2,1,0:T(8,128)}), f32[64,8,256]{2,1,0:T(8,128)}, u32[]{:S(2)}, u32[]{:S(2)}) async-start(f32[64,8,256]{2,1,0:T(8,128)} %broadcast_in_dim.25), calls=%async_computation | async-start | bytes 1048576 | tf_op jit(solution)/shard_map/all_to_all | solution.py:19
  184.3 86.0 %copy-start.1 = (bf16[128,2048]{1,0:T(8,128)(2,1)}, bf16[128,2048]{1,0:T(8,128)(2,1)S(1)}, u32[]{:S(2)}) copy-start(bf16[128,2048]{1,0:T(8,128)(2,1)S(1)} %multiply_convert_fusion.2) | copy-start | bytes 1572868
  190.3 59.0 %copy-start.39 = (bf16[1,2048,512]{2,1,0:T(8,128)(2,1)S(1)}, bf16[1,2048,512]{2,1,0:T(8,128)(2,1)}, u32[]{:S(2)}) copy-start(bf16[1,2048,512]{2,1,0:T(8,128)(2,1)} %param.34) | copy-start | bytes 6291460
  263.0 58.4 %all-to-all-start.3 = ((bf16[128,8,2048]{2,1,0:T(8,128)(2,1)}), bf16[128,8,2048]{2,1,0:T(8,128)(2,1)}, u32[]{:S(2)}, u32[]{:S(2)}) async-start(bf16[128,8,2048]{2,1,0:T(8,128)(2,1)} %convert_bitcast_fusion), calls=%async_computation.3 | async-start | bytes 8388608 | tf_op jit(solution)/shard_map/all_to_all | solution.py:165
  (21 other events, 79.9 us)
where the time goes:
time: 351 us; the launch traced here: 346 us
  local copies, waits for them, and re-layouts  128 us (36%)
  blocking collectives  63.3 us (18%)
  waiting for transfers between devices  57.3 us (16%)
  other arithmetic  46.7 us (13%)
  matrix products  28.5 us (8%)
  starting transfers between devices  21 us (6%)
    slice x52, local copies, waits for them, and re-layouts, on_device(): lax.associative_scan(combine, (jnp.exp(log_decay), update), axis=0)  67 us
    all_to_all x1, blocking collectives, on_device(): lax.all_to_all(outgoing, ('sp', 'tp'), split_axis=0, concat_axis=0, tiled...  57 us
    all_to_all x1, waiting for transfers between devices, on_device(): lax.all_to_all(jnp.dot(hidden, expert_down[0], preferred_element_type=jnp...  49.2 us
    pad x28, local copies, waits for them, and re-layouts, on_device(): lax.associative_scan(combine, (jnp.exp(log_decay), update), axis=0)  26.1 us
    add x13, other arithmetic, combine(): return (former[0] * latter[0], latter[0] * former[1] + latter[1])  15.1 us
    all_to_all x1, starting transfers between devices, sent_to_all(): lax.all_to_all(jnp.broadcast_to(x[None], (count, *x.shape)), axis, 0, 0,...  10.8 us
    dot_general x1, matrix products, on_device(): jnp.dot(hidden, expert_down[0], preferred_element_type=jnp.float32)  10 us
    all_to_all x1, waiting for transfers between devices, sent_to_all(): lax.all_to_all(jnp.broadcast_to(x[None], (count, *x.shape)), axis, 0, 0,...  8.18 us
  transfers between devices with their start and end apart: 3, of which 2 were waited for; matrix products, arithmetic and copies ran while one was open for 4% of the time, Pallas kernels for 0%

commit v1 on v0

v1 whole, which is shorter than its diff:
```python
import functools

import jax
import jax.numpy as jnp
from jax import lax
from jax.experimental import pallas as pl
from jax.experimental.pallas import tpu as pltpu
from jax.sharding import PartitionSpec as P

ALPHA = 8.0**0.25
RATE_C = 8.0
NORM_EPS = 1e-05
MESH = pl.DeviceIdType.MESH
F32, BF16 = jnp.float32, jnp.bfloat16

RING = 4
CHUNK = 16
HALO = 16
SPAN = 32


def sigmoid(x):
    return 0.5 * jnp.tanh(0.5 * x) + 0.5


def silu(x):
    return x * sigmoid(x)


def minus_expm1(y):
    series = 1.0 + y * (1.0 / 7.0)
    for n in (6, 5, 4, 3, 2):
        series = 1.0 + (y * (1.0 / n)) * series
    return jnp.where(y > -0.5, -y * series, 1.0 - jnp.exp(y))


def gelu(x):
    inner = 0.7978845608028654 * (x + 0.044715 * (x * x * x))
    return 0.5 * x * (1.0 + jnp.tanh(inner))


def dot(a, b):
    return jnp.dot(a, b, preferred_element_type=F32)


def layer_kernel(
    gate_hbm, conv_hbm, rmap_hbm, imap_hbm, outw_hbm, resid_hbm,
    sgate_hbm, sup_hbm, sdown_hbm, egate_hbm, eup_hbm, edown_hbm,
    taps_ref, rate_ref, shift_ref, gmix_ref, gout_ref,
    routes_ref, routes_t_ref, rw_ref,
    out_ref,
    gate_v, conv_v, rmap_v, imap_v, outw_v, resid_v,
    sgate_v, sup_v, sdown_v, egate_v, eup_v, edown_v,
    halo_v, ext_v, rpre_v, ipre_v, xb_v, a3, u3, g3,
    ca, ch, pa, ph, xbuf, ybuf, zbuf,
    mixed_v, theirs_v, proj_v, normed_v, shared_v, hid_v, rows_v,
    spread_v, merge_v, send_v, recv_v, res_v, ret_v,
    load_sem, halo_sem, line_send, line_recv, pair_sem,
    go_send, go_recv, back_send, back_recv,
):
    sp, tp = lax.axis_index("sp"), lax.axis_index("tp")
    x, y, z = sp % RING, (sp // RING) % RING, sp // (RING * RING)
    peers = RING * RING * RING * 2
    tokens, channels = conv_v.shape
    rows, width = normed_v.shape
    heads, bw = rmap_v.shape[0], rmap_v.shape[1]
    groups = channels // 128

    def offset_of(i):
        core, k = i % 2, i // 2
        a, b, c = k % RING, (k // RING) % RING, k // (RING * RING)
        return core, a, (a + b) % RING, (a + c) % RING

    def device_at(i, sign):
        core, dx, dy, dz = offset_of(i)
        px, py, pz = (
            (w + sign * d + RING) % RING for w, d in ((x, dx), (y, dy), (z, dz))
        )
        return {"sp": (pz * RING + py) * RING + px, "tp": (tp + core) % 2}

    barrier = pltpu.get_barrier_semaphore()

    @pl.loop(1, peers)
    def _(i):
        pl.semaphore_signal(barrier, inc=1, device_id=device_at(i, 1), device_id_type=MESH)

    half = channels
    loads = [
        (conv_hbm, conv_v), (rmap_hbm, rmap_v), (imap_hbm, imap_v), (gate_hbm, gate_v),
        (outw_hbm.at[pl.ds(pl.multiple_of(tp * half, half), half)], outw_v.at[0]),
        (outw_hbm.at[pl.ds(pl.multiple_of((1 - tp) * half, half), half)], outw_v.at[1]),
        (resid_hbm, resid_v),
        (sgate_hbm, sgate_v), (sup_hbm, sup_v), (sdown_hbm, sdown_v),
        (egate_hbm.at[0], egate_v), (eup_hbm.at[0], eup_v), (edown_hbm.at[0], edown_v),
    ]
    loads = [pltpu.make_async_copy(s, d, load_sem.at[n]) for n, (s, d) in enumerate(loads)]
    for copy in loads:
        copy.start()

    loads[0].wait()

    @pl.loop(0, tokens // 32)
    def _(b):
        at = pl.multiple_of(b * 32, 32)
        ext_v[pl.ds(HALO + at, 32), :] = conv_v[pl.ds(at, 32), :].astype(F32)

    loads[1].wait()
    loads[2].wait()

    def gates(first, count, block):
        for h in range(heads):
            cols = pl.ds(h * bw, bw)
            total = None
            for j in range(4):
                term = taps_ref[j : j + 1, cols].astype(F32) * ext_v[
                    pl.ds(HALO + first - 3 + j, count), cols
                ]
                total = term if total is None else total + term
            conv_out = total.astype(BF16)
            xb_v[0:count, :] = conv_out
            rpre_v[0:count, :] = dot(conv_out, rmap_v[h])
            ipre_v[0:count, :] = dot(conv_out, imap_v[h])
            rate = rate_ref[:, cols]

            @pl.loop(0, count // block)
            def _(b):
                at = pl.multiple_of(b * block, block)
                r = sigmoid(rpre_v[pl.ds(at, block), :])
                i = sigmoid(ipre_v[pl.ds(at, block), :])
                where = pl.ds(pl.multiple_of(first + at, 16), block)
                log_decay = rate * r + shift_ref[where, h : h + 1]
                a = jnp.exp(log_decay)
                u = jnp.sqrt(minus_expm1(2.0 * log_decay)) * i * xb_v[pl.ds(at, block), :].astype(F32)
                for g in range(bw // 128):
                    a3[h * (bw // 128) + g, where, :] = a[:, g * 128 : (g + 1) * 128]
                    u3[h * (bw // 128) + g, where, :] = u[:, g * 128 : (g + 1) * 128]

    pl.semaphore_wait(barrier, peers - 1)
    halo = pltpu.make_async_remote_copy(
        src_ref=conv_v.at[pl.ds(tokens - HALO, HALO)], dst_ref=halo_v,
        send_sem=halo_sem.at[0], recv_sem=halo_sem.at[1],
        device_id={"sp": (sp + 1) % (RING * RING * RING), "tp": tp}, device_id_type=MESH,
    )
    halo.start()
    gates(HALO, tokens - HALO, 48)
    halo.wait()
    ext_v[0:HALO, :] = jnp.where(sp == 0, 0.0, halo_v[...].astype(F32))
    gates(0, HALO, 16)

    spans = tokens // SPAN

    def walk(s, carry):
        out = []
        for g in range(groups):
            at = pl.ds(s, spans, stride=SPAN)
            a, u = a3[g, at, :], u3[g, at, :]
            out.append((carry[g][0] * a, a * carry[g][1] + u))
        return tuple(out)

    one, nought = jnp.ones((spans, 128), F32), jnp.zeros((spans, 128), F32)
    ends = lax.fori_loop(0, SPAN, walk, tuple((one, nought) for _ in range(groups)))
    for g in range(groups):
        ca[g * spans : (g + 1) * spans, :] = ends[g][0]
        ch[g * spans : (g + 1) * spans, :] = ends[g][1]
    run_a, run_h = jnp.ones((groups, 128), F32), jnp.zeros((groups, 128), F32)
    for c in range(spans):
        at = pl.ds(c, groups, stride=spans)
        pa[at, :], ph[at, :] = run_a, run_h
        a, h = ca[at, :], ch[at, :]
        run_a, run_h = run_a * a, a * run_h + h

    def exchange(n, buf, here, stride, whole_a, whole_h):
        buf[here, 0:groups, :] = whole_a
        buf[here, groups : 2 * groups, :] = whole_h
        for d in range(1, RING):
            pltpu.make_async_remote_copy(
                src_ref=buf.at[here], dst_ref=buf.at[here],
                send_sem=line_send.at[n], recv_sem=line_recv.at[n],
                device_id={"sp": sp + ((here + d) % RING - here) * stride, "tp": tp},
                device_id_type=MESH,
            ).start()

    def arrived(n, buf):
        three = buf.at[pl.ds(0, RING - 1)]
        copy = pltpu.make_async_remote_copy(
            src_ref=three, dst_ref=three, send_sem=line_send.at[n], recv_sem=line_recv.at[n],
            device_id={"sp": sp, "tp": 1 - tp}, device_id_type=MESH,
        )
        copy.wait_recv()
        copy.wait_send()

    def total_of(buf):
        a, h = buf[0, 0:groups, :], buf[0, groups : 2 * groups, :]
        for n in range(1, RING):
            na, nh = buf[n, 0:groups, :], buf[n, groups : 2 * groups, :]
            a, h = a * na, na * h + nh
        return a, h

    exchange(0, xbuf, x, 1, run_a, run_h)

    loads[3].wait()

    @pl.loop(0, tokens // 32)
    def _(b):
        at = pl.multiple_of(b * 32, 32)
        for g in range(groups):
            g3[g, pl.ds(at, 32), :] = gelu(gate_v[pl.ds(at, 32), g * 128 : (g + 1) * 128].astype(F32))

    arrived(0, xbuf)
    exchange(1, ybuf, y, RING, *total_of(xbuf))

    slots = 8
    lane_e = lax.broadcasted_iota(jnp.int32, (rows, peers), 1)
    sub_e = lax.broadcasted_iota(jnp.int32, (peers, rows), 0)
    member, member_t = jnp.zeros((rows, peers), F32), jnp.zeros((peers, rows), F32)
    weight = jnp.zeros((rows, peers), F32)
    for k in range(4):
        hit = routes_ref[:, k : k + 1] == lane_e
        member = member + jnp.where(hit, 1.0, 0.0)
        weight = weight + jnp.where(hit, rw_ref[:, k : k + 1], 0.0)
        member_t = member_t + jnp.where(routes_t_ref[k : k + 1, :] == sub_e, 1.0, 0.0)
    i0 = lax.broadcasted_iota(jnp.int32, (rows, rows), 0)
    i1 = lax.broadcasted_iota(jnp.int32, (rows, rows), 1)
    below = jnp.where(i0 > i1, 1.0, 0.0).astype(BF16)
    above = jnp.where(i0 < i1, 1.0, 0.0).astype(BF16)
    place = ((dot(below, member.astype(BF16)) + 1.0) * member).astype(BF16)
    place_t = ((dot(member_t.astype(BF16), above) + 1.0) * member_t).astype(BF16)
    weight_hi = weight.astype(BF16)
    weight_lo = (weight - weight_hi.astype(F32)).astype(BF16)

    def expert_of(i):
        core, dx, dy, dz = offset_of(i)
        chip = (((z + dz) % RING) * RING + (y + dy) % RING) * RING + (x + dx) % RING
        return chip * 2 + (tp + core) % 2

    for q in range(peers * slots // 256):
        r0 = lax.broadcasted_iota(jnp.int32, (256, peers), 0) + q * 256
        pick = jnp.where(
            expert_of(r0 // slots) == lax.broadcasted_iota(jnp.int32, (256, peers), 1), 1.0, 0.0
        ).astype(BF16)
        found = dot(pick, place_t)
        slot = (lax.broadcasted_iota(jnp.int32, (256, rows), 0) % slots + 1).astype(F32)
        spread_v[q * 256 : (q + 1) * 256, :] = jnp.where(found == slot, 1.0, 0.0).astype(BF16)
        r1 = lax.broadcasted_iota(jnp.int32, (peers, 256), 1) + q * 256
        pick_t = jnp.where(
            expert_of(r1 // slots) == lax.broadcasted_iota(jnp.int32, (peers, 256), 0), 1.0, 0.0
        ).astype(BF16)
        slot_t = (lax.broadcasted_iota(jnp.int32, (rows, 256), 1) % slots + 1).astype(F32)
        match = dot(place, pick_t) == slot_t
        merge_v[q, 0:rows, :] = jnp.where(match, dot(weight_hi, pick_t), 0.0).astype(BF16)
        merge_v[q, rows : 2 * rows, :] = jnp.where(match, dot(weight_lo, pick_t), 0.0).astype(BF16)

    arrived(1, ybuf)
    exchange(2, zbuf, z, RING * RING, *total_of(ybuf))
    arrived(2, zbuf)

    state = jnp.zeros((groups, 128), F32)
    for buf, here in ((zbuf, z), (ybuf, y), (xbuf, x)):
        for n in range(RING - 1):
            a, h = buf[n, 0:groups, :], buf[n, groups : 2 * groups, :]
            state = jnp.where(n < here, a * state + h, state)

    starts = tuple(
        pa[g * spans : (g + 1) * spans, :] * state[g : g + 1, :] + ph[g * spans : (g + 1) * spans, :]
        for g in range(groups)
    )

    def rewalk(s, carry):
        out = []
        for g in range(groups):
            at = pl.ds(s, spans, stride=SPAN)
            h = a3[g, at, :] * carry[g] + u3[g, at, :]
            u3[g, at, :] = h * g3[g, at, :]
            out.append(h)
        return tuple(out)

    lax.fori_loop(0, SPAN, rewalk, starts)

    @pl.loop(0, tokens // 32)
    def _(b):
        at = pl.multiple_of(b * 32, 32)
        for g in range(groups):
            mixed_v[pl.ds(at, 32), g * 128 : (g + 1) * 128] = u3[g, pl.ds(at, 32), :].astype(BF16)

    pair = pltpu.make_async_remote_copy(
        src_ref=mixed_v.at[pl.ds(pl.multiple_of((1 - tp) * rows, rows), rows)], dst_ref=theirs_v,
        send_sem=pair_sem.at[0], recv_sem=pair_sem.at[1],
        device_id={"sp": sp, "tp": 1 - tp}, device_id_type=MESH,
    )
    pair.start()

    tile = 256
    mine = mixed_v[pl.ds(pl.multiple_of(tp * rows, rows), rows), :]
    loads[4].wait()

    @pl.loop(0, width // tile)
    def _(n):
        cols = pl.ds(pl.multiple_of(n * tile, tile), tile)
        proj_v[:, cols] = dot(mine, outw_v[0, :, cols])

    loads[5].wait()
    loads[6].wait()
    pair.wait()
    theirs = theirs_v[...]

    @pl.loop(0, width // tile)
    def _(n):
        cols = pl.ds(pl.multiple_of(n * tile, tile), tile)
        proj_v[:, cols] = (
            ALPHA * resid_v[:, cols].astype(F32) + proj_v[:, cols] + dot(theirs, outw_v[1, :, cols])
        )

    def layer_norm(values, gains):
        center = values - jnp.mean(values, axis=-1, keepdims=True)
        spread = jnp.mean(center * center, axis=-1, keepdims=True)
        return center * lax.rsqrt(spread + NORM_EPS) * gains

    @pl.loop(0, rows // 16)
    def _(b):
        at = pl.ds(pl.multiple_of(b * 16, 16), 16)
        normed_v[at, :] = layer_norm(proj_v[at, :], gmix_ref[...]).astype(BF16)

    chunks = peers // CHUNK
    block = CHUNK * slots

    def chunk_of(ref, j):
        return ref.at[pl.ds(pl.multiple_of(j * CHUNK, CHUNK), CHUNK)]

    @pl.loop(0, chunks)
    def _(j):
        pick = spread_v[pl.ds(pl.multiple_of(j * block, block), block), :]
        for n in range(width // 512):
            part = dot(pick, normed_v[:, n * 512 : (n + 1) * 512])
            send_v[pl.ds(j * CHUNK, CHUNK), :, n * 512 : (n + 1) * 512] = part.reshape(
                CHUNK, slots, 512
            ).astype(BF16)

        @pl.loop(jnp.where(j == 0, 1, 0), CHUNK)
        def _(i):
            at = j * CHUNK + i
            pltpu.make_async_remote_copy(
                src_ref=send_v.at[at], dst_ref=recv_v.at[at],
                send_sem=go_send.at[j], recv_sem=go_recv.at[j],
                device_id=device_at(at, 1), device_id_type=MESH,
            ).start()

    def expert(x_in, gate, up, down, store):
        @pl.loop(0, gate.shape[1] // tile)
        def _(n):
            cols = pl.ds(pl.multiple_of(n * tile, tile), tile)
            hid_v[:, cols] = (silu(dot(x_in, gate[:, cols])) * dot(x_in, up[:, cols])).astype(BF16)

        hidden = hid_v[...]

        @pl.loop(0, width // tile)
        def _(n):
            cols = pl.ds(pl.multiple_of(n * tile, tile), tile)
            store(cols, dot(hidden, down[:, cols]))

    def keep_shared(cols, value):
        shared_v[:, cols] = ALPHA * normed_v[:, cols].astype(F32) + value

    loads[7].wait()
    loads[8].wait()
    loads[9].wait()
    expert(normed_v[...], sgate_v, sup_v, sdown_v, keep_shared)
    loads[10].wait()
    loads[11].wait()
    loads[12].wait()

    def waiter(ref, send, recv, j, first):
        part = ref.at[pl.ds(pl.multiple_of(j * CHUNK, CHUNK) + first, CHUNK - first)]
        return pltpu.make_async_remote_copy(
            src_ref=part, dst_ref=part, send_sem=send.at[j], recv_sem=recv.at[j],
            device_id={"sp": sp, "tp": 1 - tp}, device_id_type=MESH,
        )

    def serve(j, first):
        waiter(recv_v, go_send, go_recv, j, first).wait_recv()
        chosen = recv_v[pl.ds(j * CHUNK, CHUNK)]
        rows_v[...] = chosen.astype(F32).reshape(block, width).astype(BF16)

        def give(cols, value):
            res_v[pl.ds(j * CHUNK, CHUNK), :, cols] = value.reshape(CHUNK, slots, tile).astype(BF16)

        expert(rows_v[...], egate_v, eup_v, edown_v, give)

        @pl.loop(first, CHUNK)
        def _(i):
            at = j * CHUNK + i
            pltpu.make_async_remote_copy(
                src_ref=res_v.at[at], dst_ref=ret_v.at[at],
                send_sem=back_send.at[j], recv_sem=back_recv.at[j],
                device_id=device_at(at, -1), device_id_type=MESH,
            ).start()

    recv_v[0] = send_v[0]
    serve(0, 1)
    ret_v[0] = res_v[0]

    @pl.loop(1, chunks)
    def _(j):
        serve(j, 0)

    def merge(q, first):
        waiter(ret_v, back_send, back_recv, 2 * q, first).wait_recv()
        waiter(ret_v, back_send, back_recv, 2 * q + 1, 0).wait_recv()
        share = merge_v[q]

        @pl.loop(0, width // tile)
        def _(n):
            cols = pl.ds(pl.multiple_of(n * tile, tile), tile)
            back = ret_v[pl.ds(2 * q * CHUNK, 2 * CHUNK), :, cols]
            back = back.astype(F32).reshape(2 * block, tile).astype(BF16)
            both = dot(share, back)
            shared_v[:, cols] += both[0:rows] + both[rows : 2 * rows]

    merge(0, 1)

    @pl.loop(1, chunks // 2)
    def _(q):
        merge(q, 0)

    @pl.loop(0, rows // 16)
    def _(b):
        at = pl.ds(pl.multiple_of(b * 16, 16), 16)
        out_ref[at, :] = layer_norm(shared_v[at, :], gout_ref[...]).astype(BF16)

    waiter(send_v, go_send, go_recv, 0, 1).wait_send()
    waiter(res_v, back_send, back_recv, 0, 1).wait_send()

    @pl.loop(1, chunks)
    def _(j):
        waiter(send_v, go_send, go_recv, j, 0).wait_send()
        waiter(res_v, back_send, back_recv, j, 0).wait_send()


def on_device(
    gate_pre, conv_in, conv_taps, recur_map, input_map, rate_logit, decay_shift, out_weight,
    residual, gain_mix, routes, route_weight, shared_gate, shared_up, shared_down,
    expert_gate, expert_up, expert_down, gain_out,
):
    tokens, channels = conv_in.shape
    rows, width = residual.shape
    heads, bw = recur_map.shape[:2]
    hidden = shared_gate.shape[1]
    groups, spans, peers, slots = channels // 128, tokens // SPAN, 2 * RING**3, 8
    rate = (-RATE_C * jax.nn.softplus(-rate_logit)).reshape(1, channels)
    any_spec = pl.BlockSpec(memory_space=pl.ANY)
    vmem_spec = pl.BlockSpec(memory_space=pltpu.VMEM)
    big = [
        gate_pre, conv_in, recur_map, input_map, out_weight, residual,
        shared_gate, shared_up, shared_down, expert_gate, expert_up, expert_down,
    ]
    small = [
        conv_taps, rate, decay_shift, gain_mix.reshape(1, width), gain_out.reshape(1, width),
        routes, routes.T, route_weight,
    ]
    dma = pltpu.SemaphoreType.DMA
    chunks = peers // CHUNK
    return pl.pallas_call(
        layer_kernel,
        out_shape=jax.ShapeDtypeStruct((rows, width), BF16),
        in_specs=[any_spec] * len(big) + [vmem_spec] * len(small),
        out_specs=vmem_spec,
        scratch_shapes=[
            pltpu.VMEM((tokens, channels), BF16),
            pltpu.VMEM((tokens, channels), BF16),
            pltpu.VMEM((heads, bw, bw), BF16),
            pltpu.VMEM((heads, bw, bw), BF16),
            pltpu.VMEM((2, channels, width), BF16),
            pltpu.VMEM((rows, width), BF16),
            pltpu.VMEM((width, hidden), BF16),
            pltpu.VMEM((width, hidden), BF16),
            pltpu.VMEM((hidden, width), BF16),
            pltpu.VMEM((width, hidden), BF16),
            pltpu.VMEM((width, hidden), BF16),
            pltpu.VMEM((hidden, width), BF16),
            pltpu.VMEM((HALO, channels), BF16),
            pltpu.VMEM((HALO + tokens, channels), F32),
            pltpu.VMEM((tokens, bw), F32),
            pltpu.VMEM((tokens, bw), F32),
            pltpu.VMEM((tokens, bw), BF16),
            pltpu.VMEM((groups, tokens, 128), F32),
            pltpu.VMEM((groups, tokens, 128), F32),
            pltpu.VMEM((groups, tokens, 128), F32),
            pltpu.VMEM((groups * spans, 128), F32),
            pltpu.VMEM((groups * spans, 128), F32),
            pltpu.VMEM((groups * spans, 128), F32),
            pltpu.VMEM((groups * spans, 128), F32),
            pltpu.VMEM((RING, 2 * groups, 128), F32),
            pltpu.VMEM((RING, 2 * groups, 128), F32),
            pltpu.VMEM((RING, 2 * groups, 128), F32),
            pltpu.VMEM((tokens, channels), BF16),
            pltpu.VMEM((rows, channels), BF16),
            pltpu.VMEM((rows, width), F32),
            pltpu.VMEM((rows, width), BF16),
            pltpu.VMEM((rows, width), F32),
            pltpu.VMEM((CHUNK * slots, hidden), BF16),
            pltpu.VMEM((CHUNK * slots, width), BF16),
            pltpu.VMEM((peers * slots, rows), BF16),
            pltpu.VMEM((chunks // 2, 2 * rows, 2 * CHUNK * slots), BF16),
            pltpu.VMEM((peers, slots, width), BF16),
            pltpu.VMEM((peers, slots, width), BF16),
            pltpu.VMEM((peers, slots, width), BF16),
            pltpu.VMEM((peers, slots, width), BF16),
            dma((13,)), dma((2,)), dma((3,)), dma((3,)), dma((2,)),
            dma((chunks,)), dma((chunks,)), dma((chunks,)), dma((chunks,)),
        ],
        compiler_params=pltpu.CompilerParams(
            collective_id=0, has_side_effects=True, vmem_limit_bytes=67_043_328 - 2 * 1024 * 1024
        ),
        name="layer",
    )(*big, *small)


def solution(mesh):
    return jax.shard_map(
        on_device,
        mesh=mesh,
        in_specs=(
            P("sp", "tp"), P("sp", "tp"), P(None, "tp"), P("tp", None, None), P("tp", None, None),
            P("tp"), P("sp", "tp"), P(), P(("sp", "tp"), None), P(), P(("sp", "tp"), None),
            P(("sp", "tp"), None), P(), P(), P(), P(("sp", "tp"), None, None),
            P(("sp", "tp"), None, None), P(("sp", "tp"), None, None), P(),
        ),
        out_specs=P(("sp", "tp"), None),
        check_vma=False,
    )
```

time: 351 us -> 153 us (0.44); the launches traced: 346 us -> 153 us
  Pallas kernels: 0 us -> 145 us
  local copies, waits for them, and re-layouts: 128 us -> 6.17 us
  blocking collectives: 63.3 us -> 0 us
  waiting for transfers between devices: 57.3 us -> 0 us
  other arithmetic: 46.7 us -> 1.28 us
  matrix products: 28.5 us -> 0 us
  starting transfers between devices: 21 us -> 0 us
    pallas_call x0 -> x1, Pallas kernels: none -> 145 us  [on_device(): pl.pallas_call(layer_kernel, out_shape=jax.ShapeDtypeStruct((rows, width)...]
    slice x55 -> x0, local copies, waits for them, and re-layouts: 69.7 us -> none  [the longest x52 67 us: on_device(): lax.associative_scan(combine, (jnp.exp(log_decay), update), axis=0)]
    all_to_all x2 -> x0, blocking collectives: 63.3 us -> none  [the longest x1 57 us: on_device(): lax.all_to_all(outgoing, ('sp', 'tp'), split_axis=0, concat_axis=0, tiled...]
    all_to_all x2 -> x0, waiting for transfers between devices: 57.3 us -> none  [the longest x1 49.2 us: on_device(): lax.all_to_all(jnp.dot(hidden, expert_down[0], preferred_element_type=jnp...]
    dot_general x8 -> x0, matrix products: 28.5 us -> none  [the longest x1 10 us: on_device(): jnp.dot(hidden, expert_down[0], preferred_element_type=jnp.float32)]
    pad x28 -> x0, local copies, waits for them, and re-layouts: 26.1 us -> none  [on_device(): lax.associative_scan(combine, (jnp.exp(log_decay), update), axis=0)]
    add x29 -> x0, other arithmetic: 23.6 us -> none  [the longest x13 15.1 us: combine(): return (former[0] * latter[0], latter[0] * former[1] + latter[1])]
    all_to_all x2 -> x0, starting transfers between devices: 17.9 us -> none  [the longest x1 10.8 us: sent_to_all(): lax.all_to_all(jnp.broadcast_to(x[None], (count, *x.shape)), axis, 0, 0,...]
  transfers between devices with their start and end apart: 3 -> 0, of which waited for: 2 -> 0; matrix products, arithmetic and copies ran while one was open for 4% -> 0% of each run, Pallas kernels for 0% -> 0%
where the time goes in v1:
time: 153 us
  Pallas kernels  145 us (95%)
  local copies, waits for them, and re-layouts  6.17 us (4%)
    pallas_call x1, Pallas kernels, on_device(): pl.pallas_call(layer_kernel, out_shape=jax.ShapeDtypeStruct((rows, width)...  145 us
    unnamed x4, local copies, waits for them, and re-layouts  6.17 us

profile of v1, /device:TPU:3, one launch (start us, length us, event | category | flops | bytes accessed | tf_op | source)
XLA Modules:
  0.0 152.7 jit_solution(14483595119414229235)
XLA Ops:
  0.0 1.3 fusion
  1.3 1.4 copy.22.rw_ref
  2.7 1.4 copy.21.routes_ref
  4.1 1.5 copy.20.shift_ref
  5.6 145.2 %layer.1 = bf16[128,2048]{1,0:T(8,128)(2,1)} custom-call(bf16[256,1024]{1,0:T(8,128)(2,1)} %gate_hbm.1, bf16[256,1024]{1,0:T(8,128)(2,1)} %conv_hbm.1, bf16[4,256,256]{2,1,0:T(8,128)(2,1)} %rmap_hbm.1, bf16[4,256,256]{2,1,0:T(8,128)(2,1)} %imap_hbm.1, bf16[2048,2048]{1,0:T(8,128)(2,1)} %outw_hbm.1, bf16[128,2048]{1,0:T(8,128)(2,1)} %resid_hbm.1, ...), custom_call_target="tpu_custom_call" | custom-call | tf_op jit(solution)/shard_map/layer/pallas_call | solution.py:461
  150.8 1.9 %copy.24 = bf16[128,2048]{1,0:T(8,128)(2,1)} copy(bf16[128,2048]{1,0:T(8,128)(2,1)} %layer.1) | data formatting | bytes 1048576

commit v2 on v1

--- a/solution.py
+++ b/solution.py
@@ -17,6 +17,7 @@
 CHUNK = 16
 HALO = 16
 SPAN = 32
+PITCH = 40
 
 
 def sigmoid(x):
@@ -39,6 +40,16 @@
     return 0.5 * x * (1.0 + jnp.tanh(inner))
 
 
+def softplus(v):
+    tail = jnp.exp(-jnp.abs(v))
+    s = tail / (2.0 + tail)
+    q = s * s
+    series = 1.0 / 17.0
+    for n in (15, 13, 11, 9, 7, 5, 3):
+        series = 1.0 / n + q * series
+    return jnp.maximum(v, 0.0) + 2.0 * s * (1.0 + q * series)
+
+
 def dot(a, b):
     return jnp.dot(a, b, preferred_element_type=F32)
 
@@ -46,13 +57,13 @@
 def layer_kernel(
     gate_hbm, conv_hbm, rmap_hbm, imap_hbm, outw_hbm, resid_hbm,
     sgate_hbm, sup_hbm, sdown_hbm, egate_hbm, eup_hbm, edown_hbm,
-    taps_ref, rate_ref, shift_ref, gmix_ref, gout_ref,
-    routes_ref, routes_t_ref, rw_ref,
+    taps_hbm, logit_hbm, shift_hbm, gmix_hbm, gout_hbm, routes_hbm, rw_hbm,
     out_ref,
+    taps_ref, logit_ref, shift_t_ref, gmix_ref, gout_ref, routes_t_ref, rw_t_ref, shift_ref,
     gate_v, conv_v, rmap_v, imap_v, outw_v, resid_v,
     sgate_v, sup_v, sdown_v, egate_v, eup_v, edown_v,
     halo_v, ext_v, rpre_v, ipre_v, xb_v, a3, u3, g3,
-    ca, ch, pa, ph, xbuf, ybuf, zbuf,
+    ca, ch, pa, ph, plane_buf, zbuf,
     mixed_v, theirs_v, proj_v, normed_v, shared_v, hid_v, rows_v,
     spread_v, merge_v, send_v, recv_v, res_v, ret_v,
     load_sem, halo_sem, line_send, line_recv, pair_sem,
@@ -66,23 +77,36 @@
     heads, bw = rmap_v.shape[0], rmap_v.shape[1]
     groups = channels // 128
 
+    def wrap(v):
+        return lax.rem(v, RING)
+
+    def partners(m, sign):
+        b, c = wrap(m), lax.div(m, RING)
+        for a in range(RING):
+            px = wrap(x + sign * a + RING)
+            py = wrap(y + sign * (a + b) + 2 * RING)
+            pz = wrap(z + sign * (a + c) + 2 * RING)
+            for core in range(2):
+                other = tp if core == 0 else 1 - tp
+                yield a * 2 + core, {"sp": (pz * RING + py) * RING + px, "tp": other}
+
+    def to_partners(m, sign, act):
+        for n, device in partners(m, sign):
+            if n == 0:
+
+                @pl.when(m > 0)
+                def _():
+                    act(m * 8, device)
+
+            else:
+                act(m * 8 + n, device)
+
     def offset_of(i):
         core, k = i % 2, i // 2
         a, b, c = k % RING, (k // RING) % RING, k // (RING * RING)
         return core, a, (a + b) % RING, (a + c) % RING
 
-    def device_at(i, sign):
-        core, dx, dy, dz = offset_of(i)
-        px, py, pz = (
-            (w + sign * d + RING) % RING for w, d in ((x, dx), (y, dy), (z, dz))
-        )
-        return {"sp": (pz * RING + py) * RING + px, "tp": (tp + core) % 2}
-
     barrier = pltpu.get_barrier_semaphore()
-
-    @pl.loop(1, peers)
-    def _(i):
-        pl.semaphore_signal(barrier, inc=1, device_id=device_at(i, 1), device_id_type=MESH)
 
     half = channels
     loads = [
@@ -92,10 +116,19 @@
         (resid_hbm, resid_v),
         (sgate_hbm, sgate_v), (sup_hbm, sup_v), (sdown_hbm, sdown_v),
         (egate_hbm.at[0], egate_v), (eup_hbm.at[0], eup_v), (edown_hbm.at[0], edown_v),
+        (taps_hbm, taps_ref), (logit_hbm, logit_ref), (shift_hbm, shift_t_ref),
+        (routes_hbm, routes_t_ref), (rw_hbm, rw_t_ref), (gmix_hbm, gmix_ref), (gout_hbm, gout_ref),
     ]
     loads = [pltpu.make_async_copy(s, d, load_sem.at[n]) for n, (s, d) in enumerate(loads)]
-    for copy in loads:
+    for copy in loads[0:1] + loads[13:16] + loads[1:4] + loads[16:] + loads[4:13]:
         copy.start()
+
+    @pl.loop(0, peers // 8)
+    def _(m):
+        def greet(at, device):
+            pl.semaphore_signal(barrier, inc=1, device_id=device, device_id_type=MESH)
+
+        to_partners(m, 1, greet)
 
     loads[0].wait()
 
@@ -104,61 +137,78 @@
         at = pl.multiple_of(b * 32, 32)
         ext_v[pl.ds(HALO + at, 32), :] = conv_v[pl.ds(at, 32), :].astype(F32)
 
-    loads[1].wait()
-    loads[2].wait()
-
-    def gates(first, count, block):
-        for h in range(heads):
-            cols = pl.ds(h * bw, bw)
-            total = None
-            for j in range(4):
-                term = taps_ref[j : j + 1, cols].astype(F32) * ext_v[
-                    pl.ds(HALO + first - 3 + j, count), cols
-                ]
-                total = term if total is None else total + term
-            conv_out = total.astype(BF16)
-            xb_v[0:count, :] = conv_out
-            rpre_v[0:count, :] = dot(conv_out, rmap_v[h])
-            ipre_v[0:count, :] = dot(conv_out, imap_v[h])
-            rate = rate_ref[:, cols]
-
-            @pl.loop(0, count // block)
-            def _(b):
-                at = pl.multiple_of(b * block, block)
-                r = sigmoid(rpre_v[pl.ds(at, block), :])
-                i = sigmoid(ipre_v[pl.ds(at, block), :])
-                where = pl.ds(pl.multiple_of(first + at, 16), block)
-                log_decay = rate * r + shift_ref[where, h : h + 1]
-                a = jnp.exp(log_decay)
-                u = jnp.sqrt(minus_expm1(2.0 * log_decay)) * i * xb_v[pl.ds(at, block), :].astype(F32)
-                for g in range(bw // 128):
-                    a3[h * (bw // 128) + g, where, :] = a[:, g * 128 : (g + 1) * 128]
-                    u3[h * (bw // 128) + g, where, :] = u[:, g * 128 : (g + 1) * 128]
-
+    for n in (13, 14, 15, 1, 2):
+        loads[n].wait()
+    rate = -RATE_C * softplus(-logit_ref[...])
+    shift_rows = jnp.concatenate([shift_t_ref[...], jnp.zeros_like(shift_t_ref[...])], axis=0)
+    shift_ref[...] = shift_rows.T
+
+    def gates(h, first, count):
+        cols = slice(h * bw, (h + 1) * bw)
+        total = None
+        for j in range(4):
+            term = taps_ref[j : j + 1, cols].astype(F32) * ext_v[
+                pl.ds(HALO + first - 3 + j, count), cols
+            ]
+            total = term if total is None else total + term
+        conv_out = total.astype(BF16)
+        xb_v[0:count, :] = conv_out
+        rpre_v[0:count, :] = dot(conv_out, rmap_v[h])
+        ipre_v[0:count, :] = dot(conv_out, imap_v[h])
+
+        @pl.loop(0, count // SPAN)
+        def _(b):
+            at = pl.ds(pl.multiple_of(b * SPAN, SPAN), SPAN)
+            r = sigmoid(rpre_v[at, :])
+            i = sigmoid(ipre_v[at, :])
+            shift = shift_ref[pl.ds(pl.multiple_of(first + b * SPAN, SPAN), SPAN), h : h + 1]
+            log_decay = rate[:, cols] * r + shift
+            a = jnp.exp(log_decay)
+            u = jnp.sqrt(minus_expm1(2.0 * log_decay)) * i * xb_v[at, :].astype(F32)
+            keep = pl.ds(pl.multiple_of((first // SPAN + b) * PITCH, 8), SPAN)
+            for g in range(bw // 128):
+                a3[h * (bw // 128) + g, keep, :] = a[:, g * 128 : (g + 1) * 128]
+                u3[h * (bw // 128) + g, keep, :] = u[:, g * 128 : (g + 1) * 128]
+
+    for h in range(heads // 2):
+        gates(h, SPAN, tokens - SPAN)
     pl.semaphore_wait(barrier, peers - 1)
     halo = pltpu.make_async_remote_copy(
         src_ref=conv_v.at[pl.ds(tokens - HALO, HALO)], dst_ref=halo_v,
         send_sem=halo_sem.at[0], recv_sem=halo_sem.at[1],
-        device_id={"sp": (sp + 1) % (RING * RING * RING), "tp": tp}, device_id_type=MESH,
+        device_id={"sp": lax.rem(sp + 1, RING * RING * RING), "tp": tp}, device_id_type=MESH,
     )
     halo.start()
-    gates(HALO, tokens - HALO, 48)
+    for h in range(heads // 2, heads):
+        gates(h, SPAN, tokens - SPAN)
+
+    loads[3].wait()
+
+    @pl.loop(0, tokens // SPAN)
+    def _(b):
+        at = pl.multiple_of(b * SPAN, SPAN)
+        for g in range(groups):
+            g3[g, pl.ds(pl.multiple_of(b * PITCH, 8), SPAN), :] = gelu(
+                gate_v[pl.ds(at, SPAN), g * 128 : (g + 1) * 128].astype(F32)
+            )
+
     halo.wait()
     ext_v[0:HALO, :] = jnp.where(sp == 0, 0.0, halo_v[...].astype(F32))
-    gates(0, HALO, 16)
+    for h in range(heads):
+        gates(h, 0, SPAN)
 
     spans = tokens // SPAN
 
     def walk(s, carry):
         out = []
         for g in range(groups):
-            at = pl.ds(s, spans, stride=SPAN)
+            at = pl.ds(s, spans, stride=PITCH)
             a, u = a3[g, at, :], u3[g, at, :]
             out.append((carry[g][0] * a, a * carry[g][1] + u))
         return tuple(out)
 
     one, nought = jnp.ones((spans, 128), F32), jnp.zeros((spans, 128), F32)
-    ends = lax.fori_loop(0, SPAN, walk, tuple((one, nought) for _ in range(groups)))
+    ends = lax.fori_loop(0, SPAN, walk, tuple((one, nought) for _ in range(groups)), unroll=4)
     for g in range(groups):
         ca[g * spans : (g + 1) * spans, :] = ends[g][0]
         ch[g * spans : (g + 1) * spans, :] = ends[g][1]
@@ -170,61 +220,47 @@
         run_a, run_h = run_a * a, a * run_h + h
 
     def exchange(n, buf, here, stride, whole_a, whole_h):
+        count = buf.shape[0]
         buf[here, 0:groups, :] = whole_a
         buf[here, groups : 2 * groups, :] = whole_h
-        for d in range(1, RING):
+
+        @pl.loop(1, count)
+        def _(d):
             pltpu.make_async_remote_copy(
                 src_ref=buf.at[here], dst_ref=buf.at[here],
                 send_sem=line_send.at[n], recv_sem=line_recv.at[n],
-                device_id={"sp": sp + ((here + d) % RING - here) * stride, "tp": tp},
+                device_id={"sp": sp + (lax.rem(here + d, count) - here) * stride, "tp": tp},
                 device_id_type=MESH,
             ).start()
 
     def arrived(n, buf):
-        three = buf.at[pl.ds(0, RING - 1)]
+        others = buf.at[pl.ds(0, buf.shape[0] - 1)]
         copy = pltpu.make_async_remote_copy(
-            src_ref=three, dst_ref=three, send_sem=line_send.at[n], recv_sem=line_recv.at[n],
+            src_ref=others, dst_ref=others, send_sem=line_send.at[n], recv_sem=line_recv.at[n],
             device_id={"sp": sp, "tp": 1 - tp}, device_id_type=MESH,
         )
         copy.wait_recv()
         copy.wait_send()
 
-    def total_of(buf):
-        a, h = buf[0, 0:groups, :], buf[0, groups : 2 * groups, :]
-        for n in range(1, RING):
-            na, nh = buf[n, 0:groups, :], buf[n, groups : 2 * groups, :]
-            a, h = a * na, na * h + nh
-        return a, h
-
-    exchange(0, xbuf, x, 1, run_a, run_h)
-
-    loads[3].wait()
-
-    @pl.loop(0, tokens // 32)
-    def _(b):
-        at = pl.multiple_of(b * 32, 32)
-        for g in range(groups):
-            g3[g, pl.ds(at, 32), :] = gelu(gate_v[pl.ds(at, 32), g * 128 : (g + 1) * 128].astype(F32))
-
-    arrived(0, xbuf)
-    exchange(1, ybuf, y, RING, *total_of(xbuf))
-
+    in_plane = y * RING + x
+    exchange(0, plane_buf, in_plane, 1, run_a, run_h)
+
+    loads[16].wait()
+    loads[17].wait()
     slots = 8
-    lane_e = lax.broadcasted_iota(jnp.int32, (rows, peers), 1)
     sub_e = lax.broadcasted_iota(jnp.int32, (peers, rows), 0)
-    member, member_t = jnp.zeros((rows, peers), F32), jnp.zeros((peers, rows), F32)
-    weight = jnp.zeros((rows, peers), F32)
+    member_t, weight_t = jnp.zeros((peers, rows), F32), jnp.zeros((peers, rows), F32)
     for k in range(4):
-        hit = routes_ref[:, k : k + 1] == lane_e
-        member = member + jnp.where(hit, 1.0, 0.0)
-        weight = weight + jnp.where(hit, rw_ref[:, k : k + 1], 0.0)
-        member_t = member_t + jnp.where(routes_t_ref[k : k + 1, :] == sub_e, 1.0, 0.0)
+        hit = routes_t_ref[k : k + 1, :] == sub_e
+        member_t = member_t + jnp.where(hit, 1.0, 0.0)
+        weight_t = weight_t + jnp.where(hit, rw_t_ref[k : k + 1, :], 0.0)
     i0 = lax.broadcasted_iota(jnp.int32, (rows, rows), 0)
     i1 = lax.broadcasted_iota(jnp.int32, (rows, rows), 1)
-    below = jnp.where(i0 > i1, 1.0, 0.0).astype(BF16)
     above = jnp.where(i0 < i1, 1.0, 0.0).astype(BF16)
-    place = ((dot(below, member.astype(BF16)) + 1.0) * member).astype(BF16)
-    place_t = ((dot(member_t.astype(BF16), above) + 1.0) * member_t).astype(BF16)
+    ranks_t = (dot(member_t.astype(BF16), above) + 1.0) * member_t
+    place_t = ranks_t.astype(BF16)
+    place = ranks_t.T.astype(BF16)
+    weight = weight_t.T
     weight_hi = weight.astype(BF16)
     weight_lo = (weight - weight_hi.astype(F32)).astype(BF16)
 
@@ -233,30 +269,35 @@
         chip = (((z + dz) % RING) * RING + (y + dy) % RING) * RING + (x + dx) % RING
         return chip * 2 + (tp + core) % 2
 
-    for q in range(peers * slots // 256):
-        r0 = lax.broadcasted_iota(jnp.int32, (256, peers), 0) + q * 256
-        pick = jnp.where(
-            expert_of(r0 // slots) == lax.broadcasted_iota(jnp.int32, (256, peers), 1), 1.0, 0.0
-        ).astype(BF16)
+    wide = 256
+    slot = (lax.broadcasted_iota(jnp.int32, (wide, rows), 0) % slots + 1).astype(F32)
+    slot_t = (lax.broadcasted_iota(jnp.int32, (rows, wide), 1) % slots + 1).astype(F32)
+    step_i = lax.broadcasted_iota(jnp.int32, (wide, 1), 0)
+    step_t = lax.broadcasted_iota(jnp.int32, (1, wide), 1)
+    name_i = lax.broadcasted_iota(jnp.int32, (wide, peers), 1)
+    name_t = lax.broadcasted_iota(jnp.int32, (peers, wide), 0)
+    for q in range(peers * slots // wide):
+        pick = jnp.where(expert_of((step_i + q * wide) // slots) == name_i, 1.0, 0.0).astype(BF16)
         found = dot(pick, place_t)
-        slot = (lax.broadcasted_iota(jnp.int32, (256, rows), 0) % slots + 1).astype(F32)
-        spread_v[q * 256 : (q + 1) * 256, :] = jnp.where(found == slot, 1.0, 0.0).astype(BF16)
-        r1 = lax.broadcasted_iota(jnp.int32, (peers, 256), 1) + q * 256
-        pick_t = jnp.where(
-            expert_of(r1 // slots) == lax.broadcasted_iota(jnp.int32, (peers, 256), 0), 1.0, 0.0
-        ).astype(BF16)
-        slot_t = (lax.broadcasted_iota(jnp.int32, (rows, 256), 1) % slots + 1).astype(F32)
+        spread_v[q * wide : (q + 1) * wide, :] = jnp.where(found == slot, 1.0, 0.0).astype(BF16)
+
+    arrived(0, plane_buf)
+    plane_a, plane_h = plane_buf[0, 0:groups, :], plane_buf[0, groups : 2 * groups, :]
+    for n in range(1, RING * RING):
+        a, h = plane_buf[n, 0:groups, :], plane_buf[n, groups : 2 * groups, :]
+        plane_a, plane_h = plane_a * a, plane_h * a + h
+    exchange(1, zbuf, z, RING * RING, plane_a, plane_h)
+    for q in range(peers * slots // wide):
+        pick_t = jnp.where(expert_of((step_t + q * wide) // slots) == name_t, 1.0, 0.0).astype(BF16)
         match = dot(place, pick_t) == slot_t
         merge_v[q, 0:rows, :] = jnp.where(match, dot(weight_hi, pick_t), 0.0).astype(BF16)
         merge_v[q, rows : 2 * rows, :] = jnp.where(match, dot(weight_lo, pick_t), 0.0).astype(BF16)
 
-    arrived(1, ybuf)
-    exchange(2, zbuf, z, RING * RING, *total_of(ybuf))
-    arrived(2, zbuf)
+    arrived(1, zbuf)
 
     state = jnp.zeros((groups, 128), F32)
-    for buf, here in ((zbuf, z), (ybuf, y), (xbuf, x)):
-        for n in range(RING - 1):
+    for buf, here in ((zbuf, z), (plane_buf, in_plane)):
+        for n in range(buf.shape[0] - 1):
             a, h = buf[n, 0:groups, :], buf[n, groups : 2 * groups, :]
             state = jnp.where(n < here, a * state + h, state)
 
@@ -268,26 +309,30 @@
     def rewalk(s, carry):
         out = []
         for g in range(groups):
-            at = pl.ds(s, spans, stride=SPAN)
+            at = pl.ds(s, spans, stride=PITCH)
             h = a3[g, at, :] * carry[g] + u3[g, at, :]
             u3[g, at, :] = h * g3[g, at, :]
             out.append(h)
         return tuple(out)
 
-    lax.fori_loop(0, SPAN, rewalk, starts)
-
-    @pl.loop(0, tokens // 32)
-    def _(b):
-        at = pl.multiple_of(b * 32, 32)
-        for g in range(groups):
-            mixed_v[pl.ds(at, 32), g * 128 : (g + 1) * 128] = u3[g, pl.ds(at, 32), :].astype(BF16)
-
+    lax.fori_loop(0, SPAN, rewalk, starts, unroll=4)
+
+    def round_rows(first):
+        @pl.loop(0, rows // SPAN)
+        def _(b):
+            at = pl.ds(pl.multiple_of(first + b * SPAN, SPAN), SPAN)
+            keep = pl.ds(pl.multiple_of((first // SPAN + b) * PITCH, 8), SPAN)
+            for g in range(groups):
+                mixed_v[at, g * 128 : (g + 1) * 128] = u3[g, keep, :].astype(BF16)
+
+    round_rows((1 - tp) * rows)
     pair = pltpu.make_async_remote_copy(
         src_ref=mixed_v.at[pl.ds(pl.multiple_of((1 - tp) * rows, rows), rows)], dst_ref=theirs_v,
         send_sem=pair_sem.at[0], recv_sem=pair_sem.at[1],
         device_id={"sp": sp, "tp": 1 - tp}, device_id_type=MESH,
     )
     pair.start()
+    round_rows(tp * rows)
 
     tile = 256
     mine = mixed_v[pl.ds(pl.multiple_of(tp * rows, rows), rows), :]
@@ -314,6 +359,9 @@
         center = values - jnp.mean(values, axis=-1, keepdims=True)
         spread = jnp.mean(center * center, axis=-1, keepdims=True)
         return center * lax.rsqrt(spread + NORM_EPS) * gains
+
+    loads[18].wait()
+    loads[19].wait()
 
     @pl.loop(0, rows // 16)
     def _(b):
@@ -335,14 +383,16 @@
                 CHUNK, slots, 512
             ).astype(BF16)
 
-        @pl.loop(jnp.where(j == 0, 1, 0), CHUNK)
-        def _(i):
-            at = j * CHUNK + i
+        def give(at, device):
             pltpu.make_async_remote_copy(
                 src_ref=send_v.at[at], dst_ref=recv_v.at[at],
                 send_sem=go_send.at[j], recv_sem=go_recv.at[j],
-                device_id=device_at(at, 1), device_id_type=MESH,
+                device_id=device, device_id_type=MESH,
             ).start()
+
+        @pl.loop(0, CHUNK // 8)
+        def _(half):
+            to_partners(j * (CHUNK // 8) + half, 1, give)
 
     def expert(x_in, gate, up, down, store):
         @pl.loop(0, gate.shape[1] // tile)
@@ -385,14 +435,16 @@
 
         expert(rows_v[...], egate_v, eup_v, edown_v, give)
 
-        @pl.loop(first, CHUNK)
-        def _(i):
-            at = j * CHUNK + i
+        def give_back(at, device):
             pltpu.make_async_remote_copy(
                 src_ref=res_v.at[at], dst_ref=ret_v.at[at],
                 send_sem=back_send.at[j], recv_sem=back_recv.at[j],
-                device_id=device_at(at, -1), device_id_type=MESH,
+                device_id=device, device_id_type=MESH,
             ).start()
+
+        @pl.loop(0, CHUNK // 8)
+        def _(half):
+            to_partners(j * (CHUNK // 8) + half, -1, give_back)
 
     recv_v[0] = send_v[0]
     serve(0, 1)
@@ -445,7 +497,6 @@
     heads, bw = recur_map.shape[:2]
     hidden = shared_gate.shape[1]
     groups, spans, peers, slots = channels // 128, tokens // SPAN, 2 * RING**3, 8
-    rate = (-RATE_C * jax.nn.softplus(-rate_logit)).reshape(1, channels)
     any_spec = pl.BlockSpec(memory_space=pl.ANY)
     vmem_spec = pl.BlockSpec(memory_space=pltpu.VMEM)
     big = [
@@ -453,17 +504,19 @@
         shared_gate, shared_up, shared_down, expert_gate, expert_up, expert_down,
     ]
     small = [
-        conv_taps, rate, decay_shift, gain_mix.reshape(1, width), gain_out.reshape(1, width),
-        routes, routes.T, route_weight,
+        conv_taps, rate_logit.reshape(1, channels), decay_shift.T, gain_mix.reshape(1, width),
+        gain_out.reshape(1, width), routes.T, route_weight.T,
     ]
     dma = pltpu.SemaphoreType.DMA
     chunks = peers // CHUNK
     return pl.pallas_call(
         layer_kernel,
         out_shape=jax.ShapeDtypeStruct((rows, width), BF16),
-        in_specs=[any_spec] * len(big) + [vmem_spec] * len(small),
+        in_specs=[any_spec] * (len(big) + len(small)),
         out_specs=vmem_spec,
-        scratch_shapes=[
+        scratch_shapes=[pltpu.VMEM(v.shape, v.dtype) for v in small]
+        + [
+            pltpu.VMEM((tokens, 8), F32),
             pltpu.VMEM((tokens, channels), BF16),
             pltpu.VMEM((tokens, channels), BF16),
             pltpu.VMEM((heads, bw, bw), BF16),
@@ -481,15 +534,14 @@
             pltpu.VMEM((tokens, bw), F32),
             pltpu.VMEM((tokens, bw), F32),
             pltpu.VMEM((tokens, bw), BF16),
-            pltpu.VMEM((groups, tokens, 128), F32),
-            pltpu.VMEM((groups, tokens, 128), F32),
-            pltpu.VMEM((groups, tokens, 128), F32),
+            pltpu.VMEM((groups, spans * PITCH, 128), F32),
+            pltpu.VMEM((groups, spans * PITCH, 128), F32),
+            pltpu.VMEM((groups, spans * PITCH, 128), F32),
             pltpu.VMEM((groups * spans, 128), F32),
             pltpu.VMEM((groups * spans, 128), F32),
             pltpu.VMEM((groups * spans, 128), F32),
             pltpu.VMEM((groups * spans, 128), F32),
-            pltpu.VMEM((RING, 2 * groups, 128), F32),
-            pltpu.VMEM((RING, 2 * groups, 128), F32),
+            pltpu.VMEM((RING * RING, 2 * groups, 128), F32),
             pltpu.VMEM((RING, 2 * groups, 128), F32),
             pltpu.VMEM((tokens, channels), BF16),
             pltpu.VMEM((rows, channels), BF16),
@@ -504,11 +556,11 @@
             pltpu.VMEM((peers, slots, width), BF16),
             pltpu.VMEM((peers, slots, width), BF16),
             pltpu.VMEM((peers, slots, width), BF16),
-            dma((13,)), dma((2,)), dma((3,)), dma((3,)), dma((2,)),
+            dma((20,)), dma((2,)), dma((2,)), dma((2,)), dma((2,)),
             dma((chunks,)), dma((chunks,)), dma((chunks,)), dma((chunks,)),
         ],
         compiler_params=pltpu.CompilerParams(
-            collective_id=0, has_side_effects=True, vmem_limit_bytes=67_043_328 - 2 * 1024 * 1024
+            collective_id=0, has_side_effects=True, vmem_limit_bytes=52 * 1024 * 1024
         ),
         name="layer",
     )(*big, *small)

time: 153 us -> 140 us (0.915)
  Pallas kernels: 145 us -> 132 us
  local copies, waits for them, and re-layouts: 6.17 us -> 7.7 us
    pallas_call x1, Pallas kernels: 145 us -> 132 us  [on_device(): pl.pallas_call(layer_kernel, out_shape=jax.ShapeDtypeStruct((rows, width)...]
    unnamed x4 -> x19, local copies, waits for them, and re-layouts: 6.17 us -> 7.7 us
where the time goes in v2:
time: 140 us
  Pallas kernels  132 us (94%)
  local copies, waits for them, and re-layouts  7.7 us (6%)
    pallas_call x1, Pallas kernels, on_device(): pl.pallas_call(layer_kernel, out_shape=jax.ShapeDtypeStruct((rows, width)...  132 us
    unnamed x19, local copies, waits for them, and re-layouts  7.7 us

profile of v2, /device:TPU:3, one launch (start us, length us, event | category | flops | bytes accessed | tf_op | source)
XLA Modules:
  0.0 139.6 jit_solution(10311741483368786093)
XLA Ops:
  0.0 0.0 copy-start
  0.0 1.0 copy-done
  1.0 0.0 copy-start.1
  1.0 1.0 copy-done.1
  2.1 0.0 copy-start.2
  2.1 0.7 copy-done.2
  2.8 0.0 copy-start.3
  2.8 0.7 copy-done.3
  3.5 0.0 copy-start.4
  3.5 0.7 copy-done.4
  4.2 0.0 copy-start.5
  4.2 0.7 copy-done.5
  4.9 0.0 copy-start.6
  4.9 0.7 copy-done.6
  5.6 0.0 copy-start.7
  5.6 0.7 copy-done.7
  6.2 0.0 copy-start.8
  6.2 0.7 copy-done.8
  6.9 131.9 %layer.1 = bf16[128,2048]{1,0:T(8,128)(2,1)S(1)} custom-call(bf16[256,1024]{1,0:T(8,128)(2,1)S(1)} %copy-done, bf16[256,1024]{1,0:T(8,128)(2,1)S(1)} %copy-done.1, bf16[4,256,256]{2,1,0:T(8,128)(2,1)} %rmap_hbm.1, bf16[4,256,256]{2,1,0:T(8,128)(2,1)} %imap_hbm.1, bf16[2048,2048]{1,0:T(8,128)(2,1)} %outw_hbm.1, bf16[128,2048]{1,0:T(8,128)(2,1)} %resid_hbm.1, ...), custom_call_target="tpu_custom_call" | custom-call | tf_op jit(solution)/shard_map/layer/pallas_call | solution.py:512
  138.8 0.8 copy.21
Async XLA Ops:
  0.0 1.0 copy-start
  1.0 1.0 copy-start.1
  2.1 0.7 copy-start.2
  2.8 0.7 copy-start.3
  3.5 0.7 copy-start.4
  4.2 0.7 copy-start.5
  4.9 0.7 copy-start.6
  5.6 0.7 copy-start.7
  6.2 0.7 copy-start.8

commit v3 on v2

--- a/solution.py
+++ b/solution.py
@@ -120,7 +120,7 @@
         (routes_hbm, routes_t_ref), (rw_hbm, rw_t_ref), (gmix_hbm, gmix_ref), (gout_hbm, gout_ref),
     ]
     loads = [pltpu.make_async_copy(s, d, load_sem.at[n]) for n, (s, d) in enumerate(loads)]
-    for copy in loads[0:1] + loads[13:16] + loads[1:4] + loads[16:] + loads[4:13]:
+    for copy in loads[0:1] + loads[13:16] + loads[1:4] + loads[16:] + loads[4:5] + loads[6:7] + loads[5:6] + loads[7:13]:
         copy.start()
 
     @pl.loop(0, peers // 8)
@@ -337,23 +337,21 @@
     tile = 256
     mine = mixed_v[pl.ds(pl.multiple_of(tp * rows, rows), rows), :]
     loads[4].wait()
+    loads[6].wait()
 
     @pl.loop(0, width // tile)
     def _(n):
         cols = pl.ds(pl.multiple_of(n * tile, tile), tile)
-        proj_v[:, cols] = dot(mine, outw_v[0, :, cols])
+        proj_v[:, cols] = ALPHA * resid_v[:, cols].astype(F32) + dot(mine, outw_v[0, :, cols])
 
     loads[5].wait()
-    loads[6].wait()
     pair.wait()
     theirs = theirs_v[...]
 
     @pl.loop(0, width // tile)
     def _(n):
         cols = pl.ds(pl.multiple_of(n * tile, tile), tile)
-        proj_v[:, cols] = (
-            ALPHA * resid_v[:, cols].astype(F32) + proj_v[:, cols] + dot(theirs, outw_v[1, :, cols])
-        )
+        proj_v[:, cols] += dot(theirs, outw_v[1, :, cols])
 
     def layer_norm(values, gains):
         center = values - jnp.mean(values, axis=-1, keepdims=True)
@@ -363,7 +361,7 @@
     loads[18].wait()
     loads[19].wait()
 
-    @pl.loop(0, rows // 16)
+    @pl.loop(0, rows // 16, unroll=4)
     def _(b):
         at = pl.ds(pl.multiple_of(b * 16, 16), 16)
         normed_v[at, :] = layer_norm(proj_v[at, :], gmix_ref[...]).astype(BF16)
@@ -473,7 +471,7 @@
     def _(q):
         merge(q, 0)
 
-    @pl.loop(0, rows // 16)
+    @pl.loop(0, rows // 16, unroll=4)
     def _(b):
         at = pl.ds(pl.multiple_of(b * 16, 16), 16)
         out_ref[at, :] = layer_norm(shared_v[at, :], gout_ref[...]).astype(BF16)
@@ -563,7 +561,7 @@
             collective_id=0, has_side_effects=True, vmem_limit_bytes=52 * 1024 * 1024
         ),
         name="layer",
-    )(*big, *small)
+    )(*(pltpu.with_memory_space_constraint(v, pltpu.HBM) for v in (*big, *small)))
 
 
 def solution(mesh):

time: 140 us -> 131 us (0.936)
  local copies, waits for them, and re-layouts: 7.7 us -> 0.8 us
  Pallas kernels: 132 us -> 130 us
    unnamed x19 -> x1, local copies, waits for them, and re-layouts: 7.7 us -> 0.8 us
    pallas_call x1, Pallas kernels: 132 us -> 130 us  [on_device(): pl.pallas_call(layer_kernel, out_shape=jax.ShapeDtypeStruct((rows, width)...]
where the time goes in v3:
time: 131 us
  Pallas kernels  130 us (99%)
    pallas_call x1, Pallas kernels, on_device(): pl.pallas_call(layer_kernel, out_shape=jax.ShapeDtypeStruct((rows, width)...  130 us

profile of v3, /device:TPU:3, one launch (start us, length us, event | category | flops | bytes accessed | tf_op | source)
XLA Modules:
  0.0 130.8 jit_solution(13088991155824631033)
XLA Ops:
  0.0 130.0 %layer.1 = bf16[128,2048]{1,0:T(8,128)(2,1)S(1)} custom-call(bf16[256,1024]{1,0:T(8,128)(2,1)} %gate_hbm.1, bf16[256,1024]{1,0:T(8,128)(2,1)} %conv_hbm.1, bf16[4,256,256]{2,1,0:T(8,128)(2,1)} %rmap_hbm.1, bf16[4,256,256]{2,1,0:T(8,128)(2,1)} %imap_hbm.1, bf16[2048,2048]{1,0:T(8,128)(2,1)} %outw_hbm.1, bf16[128,2048]{1,0:T(8,128)(2,1)} %resid_hbm.1, ...), custom_call_target="tpu_custom_call" | custom-call | tf_op jit(solution)/shard_map/layer/pallas_call | solution.py:510
  130.1 0.8 copy.21

commit v4 on v3

--- a/solution.py
+++ b/solution.py
@@ -80,18 +80,22 @@
     def wrap(v):
         return lax.rem(v, RING)
 
-    def partners(m, sign):
+    turn = 1 - 2 * tp
+
+    def partners(m, signs):
         b, c = wrap(m), lax.div(m, RING)
         for a in range(RING):
-            px = wrap(x + sign * a + RING)
-            py = wrap(y + sign * (a + b) + 2 * RING)
-            pz = wrap(z + sign * (a + c) + 2 * RING)
-            for core in range(2):
+            for core, sign in enumerate(signs):
+                px = wrap(x + sign * a + RING)
+                py = wrap(y + sign * (a + b) + 2 * RING)
+                pz = wrap(z + sign * (a + c) + 2 * RING)
                 other = tp if core == 0 else 1 - tp
                 yield a * 2 + core, {"sp": (pz * RING + py) * RING + px, "tp": other}
 
-    def to_partners(m, sign, act):
-        for n, device in partners(m, sign):
+    ahead, behind = (turn, turn), (-turn, turn)
+
+    def to_partners(m, signs, act):
+        for n, device in partners(m, signs):
             if n == 0:
 
                 @pl.when(m > 0)
@@ -120,15 +124,15 @@
         (routes_hbm, routes_t_ref), (rw_hbm, rw_t_ref), (gmix_hbm, gmix_ref), (gout_hbm, gout_ref),
     ]
     loads = [pltpu.make_async_copy(s, d, load_sem.at[n]) for n, (s, d) in enumerate(loads)]
-    for copy in loads[0:1] + loads[13:16] + loads[1:4] + loads[16:] + loads[4:5] + loads[6:7] + loads[5:6] + loads[7:13]:
-        copy.start()
-
     @pl.loop(0, peers // 8)
     def _(m):
         def greet(at, device):
             pl.semaphore_signal(barrier, inc=1, device_id=device, device_id_type=MESH)
 
-        to_partners(m, 1, greet)
+        to_partners(m, ahead, greet)
+
+    for copy in loads[0:1] + loads[13:16] + loads[1:4] + loads[16:] + loads[4:5] + loads[6:7] + loads[5:6] + loads[7:13]:
+        copy.start()
 
     loads[0].wait()
 
@@ -266,7 +270,8 @@
 
     def expert_of(i):
         core, dx, dy, dz = offset_of(i)
-        chip = (((z + dz) % RING) * RING + (y + dy) % RING) * RING + (x + dx) % RING
+        chip = ((z + turn * dz + RING) % RING) * RING + (y + turn * dy + RING) % RING
+        chip = chip * RING + (x + turn * dx + RING) % RING
         return chip * 2 + (tp + core) % 2
 
     wide = 256
@@ -390,7 +395,7 @@
 
         @pl.loop(0, CHUNK // 8)
         def _(half):
-            to_partners(j * (CHUNK // 8) + half, 1, give)
+            to_partners(j * (CHUNK // 8) + half, ahead, give)
 
     def expert(x_in, gate, up, down, store):
         @pl.loop(0, gate.shape[1] // tile)
@@ -442,7 +447,7 @@
 
         @pl.loop(0, CHUNK // 8)
         def _(half):
-            to_partners(j * (CHUNK // 8) + half, -1, give_back)
+            to_partners(j * (CHUNK // 8) + half, behind, give_back)
 
     recv_v[0] = send_v[0]
     serve(0, 1)

time: 131 us -> 129 us (0.985)
  Pallas kernels: 130 us -> 128 us
    pallas_call x1, Pallas kernels: 130 us -> 128 us  [on_device(): pl.pallas_call(layer_kernel, out_shape=jax.ShapeDtypeStruct((rows, width)...]
where the time goes in v4:
time: 129 us
  Pallas kernels  128 us (99%)
    pallas_call x1, Pallas kernels, on_device(): pl.pallas_call(layer_kernel, out_shape=jax.ShapeDtypeStruct((rows, width)...  128 us

profile of v4, /device:TPU:3, one launch (start us, length us, event | category | flops | bytes accessed | tf_op | source)
XLA Modules:
  0.0 129.3 jit_solution(7065037374156962493)
XLA Ops:
  0.0 128.5 %layer.1 = bf16[128,2048]{1,0:T(8,128)(2,1)S(1)} custom-call(bf16[256,1024]{1,0:T(8,128)(2,1)} %gate_hbm.1, bf16[256,1024]{1,0:T(8,128)(2,1)} %conv_hbm.1, bf16[4,256,256]{2,1,0:T(8,128)(2,1)} %rmap_hbm.1, bf16[4,256,256]{2,1,0:T(8,128)(2,1)} %imap_hbm.1, bf16[2048,2048]{1,0:T(8,128)(2,1)} %outw_hbm.1, bf16[128,2048]{1,0:T(8,128)(2,1)} %resid_hbm.1, ...), custom_call_target="tpu_custom_call" | custom-call | tf_op jit(solution)/shard_map/layer/pallas_call | solution.py:515
  128.5 0.8 copy.21
